TPU v7x, 32 devices: a whole 2x2x4 slice. The times are simulated.
32 devices in a mesh: ep: 8 (over z, x), tp: 4 (over y, core).
Axes of the slice: x: 2, y: 2, z: 4, core: 2. Of those that a mesh axis runs over, the one named last changes fastest.
Arguments:
- queries: bfloat16 [2048, 2048], P('ep', 'tp'), may hold values from -9 to 9
- key_rows: bfloat16 [2048, 2048], P('ep', 'tp'), may hold values from -9 to 9
- values: bfloat16 [2048, 2048], P('ep', 'tp'), may hold values from -6 to 6
- second_scale: float32 [16], P('tp'), may hold values from 0.3 to 0.8
- head_gain: float32 [128], replicated, may hold values from 0.1 to 1.9
- out_weight: bfloat16 [2048, 2048], P(None, 'tp'), may hold values from -0.125 to 0.125
- routed_in: bfloat16 [2048, 2048], P('ep'), may hold values from -6 to 6
- routed_gain: float32 [2048], replicated, may hold values from 0.1 to 1.9
- expert_ids: int32 [2048, 2], P('ep'), may hold values from 0 to 7, all different within a row; in each aligned block of 256 rows (0 to 255, 256 to 511, ...) at most 128 rows name the same one
- group_logits: float32 [2048, 2], P('ep'), may hold values from -6 to 6
- inner_logits: float32 [2048, 2], P('ep'), may hold values from -6 to 6
- gate_weight: bfloat16 [8, 2048, 4096], P('ep', None, 'tp'), may hold values from -0.125 to 0.125
- up_weight: bfloat16 [8, 2048, 4096], P('ep', None, 'tp'), may hold values from -0.125 to 0.125
- down_weight: bfloat16 [8, 4096, 2048], P('ep', 'tp'), may hold values from -0.09375 to 0.09375
Outputs:
- mixer_out: bfloat16 [2048, 2048], P('ep', 'tp')
- routed_out: bfloat16 [2048, 2048], P('ep', 'tp')
Inputs may be any that keep to these rules, and one draw needn't show every extreme that they name: `expert_ids`: the two ids of a row differ. In the rows of one device (aligned blocks of 256 rows) no expert is named by more than 128 rows, a bound that some block reaches.
All inputs are finite; a program needn't handle non-finite values.
Results may differ from a plain program's by a relative error of at most 0.018.
Values may be sent and summed in bfloat16 or wider, within the bound.
No kernel may reach another device: no remote copies, remote signals or barrier semaphores. Data moves between devices by JAX's collectives and lax.ppermute only.
A program may use at most 128 MiB of HBM per device.

v0:
```python
import math
import jax
import jax.numpy as jnp
from jax import lax
from jax.sharding import PartitionSpec as P

GROUP_SIZE = 4
EPSILON = 1e-05
LOWEST = -1e30


def token_mixer(queries, key_rows, values, second_scale, head_gain, out_weight):
    row_count = queries.shape[0]
    local_heads = second_scale.shape[0]
    qk_size = queries.shape[1] // (2 * local_heads)
    value_size = values.shape[1] // local_heads
    first_pos = lax.axis_index("ep") * row_count
    query_pos = first_pos + jnp.arange(row_count, dtype=jnp.int32)
    last_pos = first_pos + row_count - 1
    query_four = queries.reshape(row_count, local_heads, 2, qk_size)
    score_scale = qk_size ** (-0.5)
    initial = (
        jnp.full((row_count, local_heads, 2), LOWEST, jnp.float32),
        jnp.zeros((row_count, local_heads, 2), jnp.float32),
        jnp.zeros((row_count, local_heads, 2, value_size), jnp.float32),
    )
    state_now = initial
    key_piece = lax.all_gather(key_rows, "ep", axis=0, tiled=True)
    value_piece = lax.all_gather(values, "ep", axis=0, tiled=True)
    piece_count = key_piece.shape[0]
    block_width = math.gcd(piece_count, 512)
    blocks = piece_count // block_width
    key_blocks = key_piece.reshape(blocks, block_width, local_heads, 2, qk_size)
    value_blocks = value_piece.reshape(blocks, block_width, local_heads, value_size)

    def update(state_inner, block_index):
        key_start = block_index * block_width

        def attend(inner_state):
            running_max, denominator, weighted = inner_state
            scores = (
                jnp.einsum(
                    "qhmd,khmd->qhmk",
                    query_four,
                    key_blocks[block_index],
                    preferred_element_type=jnp.float32,
                )
                * score_scale
            )
            key_pos = key_start + jnp.arange(block_width, dtype=jnp.int32)
            visible = (query_pos[:, None] >= key_pos[None, :])[:, None, None, :]
            scores = jnp.where(visible, scores, LOWEST)
            new_max = jnp.maximum(running_max, jnp.max(scores, axis=-1))
            exp_terms = jnp.where(visible, jnp.exp(scores - new_max[..., None]), 0.0)
            factor = jnp.exp(running_max - new_max)
            denominator = denominator * factor + jnp.sum(exp_terms, axis=-1)
            weighted = weighted * factor[..., None] + jnp.einsum(
                "qhmk,khe->qhme",
                exp_terms.astype(jnp.bfloat16),
                value_blocks[block_index],
                preferred_element_type=jnp.float32,
            )
            return (new_max, denominator, weighted)

        return (
            lax.cond(key_start <= last_pos, attend, lambda inner_state: inner_state, state_inner),
            None,
        )

    state_now, _ = lax.scan(update, state_now, jnp.arange(blocks, dtype=jnp.int32))
    running_max, denominator, weighted = state_now
    mapped = weighted / denominator[..., None]
    difference = mapped[:, :, 0] - second_scale[None, :, None] * mapped[:, :, 1]
    inv_norm = lax.rsqrt(jnp.mean(difference * difference, axis=-1, keepdims=True) + EPSILON)
    head_out = (
        (difference * inv_norm * head_gain)
        .astype(jnp.bfloat16)
        .reshape(row_count, local_heads * value_size)
    )
    mixed = jnp.dot(
        lax.all_gather(head_out, "tp", axis=1, tiled=True),
        out_weight,
        preferred_element_type=jnp.float32,
    )
    return mixed.astype(jnp.bfloat16)


def expert_block(
    routed_in,
    routed_gain,
    expert_ids,
    group_logits,
    inner_logits,
    gate_weight,
    up_weight,
    down_weight,
):
    token_count = routed_in.shape[0]
    chosen = expert_ids.shape[1]
    ep_size = lax.axis_size("ep")
    capacity = 2 * chosen * token_count // ep_size
    source = routed_in.astype(jnp.float32)
    normed = (
        source
        * lax.rsqrt(jnp.mean(source * source, axis=-1, keepdims=True) + EPSILON)
        * routed_gain
    ).astype(jnp.bfloat16)
    flat_ids = expert_ids.reshape(-1)
    picked = (flat_ids[:, None] == jnp.arange(ep_size, dtype=jnp.int32)[None, :]).astype(jnp.int32)
    slot_index = jnp.sum(jnp.cumsum(picked, axis=0) * picked, axis=1) - 1
    place_index = flat_ids * capacity + slot_index
    owner_row = jnp.arange(token_count * chosen, dtype=jnp.int32) // chosen
    slot_rows = jnp.zeros((ep_size * capacity,), jnp.int32).at[place_index].set(owner_row)
    outgoing = normed[slot_rows].reshape(ep_size, capacity, normed.shape[1])
    gate_local = gate_weight[0]
    up_local = up_weight[0]
    down_local = down_weight[0]
    columns = outgoing.shape[2] // lax.axis_size("tp")
    own_columns = lax.dynamic_slice_in_dim(outgoing, lax.axis_index("tp") * columns, columns, 2)
    arrived = lax.all_to_all(own_columns, "ep", split_axis=0, concat_axis=0, tiled=True)
    experts_arrived = lax.all_gather(arrived, "tp", axis=2, tiled=True)
    stacked = experts_arrived.reshape(-1, experts_arrived.shape[2])
    gate_act = jnp.dot(stacked, gate_local, preferred_element_type=jnp.float32)
    up_act = jnp.dot(stacked, up_local, preferred_element_type=jnp.float32)
    hidden = (jax.nn.silu(gate_act) * up_act).astype(jnp.bfloat16)
    partial_value = jnp.dot(hidden, down_local, preferred_element_type=jnp.float32)
    partial_value = partial_value.reshape(
        experts_arrived.shape[0], experts_arrived.shape[1], partial_value.shape[1]
    )
    answered = lax.psum_scatter(
        partial_value.astype(jnp.bfloat16), "tp", scatter_dimension=2, tiled=True
    )
    returned = lax.all_to_all(answered, "ep", split_axis=0, concat_axis=0, tiled=True)
    pair_out = returned.reshape(ep_size * capacity, returned.shape[2])[place_index]
    pair_out = pair_out.reshape(token_count, chosen, returned.shape[2])
    group_prob = jax.nn.softmax(group_logits, axis=-1)
    member = (
        expert_ids[..., None] // GROUP_SIZE == jnp.arange(group_logits.shape[1], dtype=jnp.int32)
    ).astype(jnp.float32)
    group_pick = jnp.sum(group_prob[:, None, :] * member, axis=-1)
    route_weight = group_pick * jax.nn.softmax(inner_logits, axis=-1)
    return jnp.sum(route_weight[..., None] * pair_out.astype(jnp.float32), axis=1).astype(
        jnp.bfloat16
    )


def local(
    queries,
    key_rows,
    values,
    second_scale,
    head_gain,
    out_weight,
    routed_in,
    routed_gain,
    expert_ids,
    group_logits,
    inner_logits,
    gate_weight,
    up_weight,
    down_weight,
):
    mixer_out = token_mixer(queries, key_rows, values, second_scale, head_gain, out_weight)
    routed_out = expert_block(
        routed_in,
        routed_gain,
        expert_ids,
        group_logits,
        inner_logits,
        gate_weight,
        up_weight,
        down_weight,
    )
    return (mixer_out, routed_out)


def solution(mesh):
    return jax.shard_map(
        local,
        mesh=mesh,
        in_specs=(
            P("ep", "tp"),
            P("ep", "tp"),
            P("ep", "tp"),
            P("tp"),
            P(),
            P(None, "tp"),
            P("ep", None),
            P(),
            P("ep", None),
            P("ep", None),
            P("ep", None),
            P("ep", None, "tp"),
            P("ep", None, "tp"),
            P("ep", "tp", None),
        ),
        out_specs=(P("ep", "tp"), P("ep", "tp")),
        check_vma=False,
    )
```

profile of v0, /device:TPU:0, one launch (start us, length us, event | category | flops | bytes accessed | tf_op | source)
XLA Modules:
  0.0 282.8 jit_solution(2242656608701986712)
XLA Ops:
  7.2 1.4 and_select_fusion
  9.8 1.5 fusion.35
  13.1 2.4 scatter_custom_fusion
  15.6 1.5 fusion.37
  17.1 6.0 %gather_fusion = bf16[1024,2048]{1,0:T(8,128)(2,1)} fusion(bf16[256,2048]{1,0:T(8,128)(2,1)S(1)} %fusion.37, s32[1024]{0:T(1024)S(1)} %fusion.46), kind=kCustom, calls=%fused_computation | custom fusion | bytes 8392704 | tf_op jit(solution)/shard_map/gather | solution.py:114
  23.2 1.3 constant_dynamic-slice_fusion
  24.5 32.9 %all_to_all.10 = bf16[8,128,512]{2,1,0:T(8,128)(2,1)} all-to-all(bf16[8,128,512]{2,1,0:T(8,128)(2,1)S(1)} %constant_dynamic-slice_fusion), channel_id=1, replica_groups=mesh['ep'=8,'tp'=4] {'ep'}, dimensions={0} | all-to-all | bytes 2097152 | tf_op jit(solution)/shard_map/all_to_all | solution.py:120
  59.0 32.1 %all-gather.11.cloned.1.call-done = bf16[8,128,2048]{2,1,0:T(8,128)(2,1)} async-done(((bf16[8,128,512]{2,1,0:T(8,128)(2,1)}), bf16[8,128,2048]{2,1,0:T(8,128)(2,1)}) %all-gather.11.cloned.1.call-update) | async-done | bytes 4194320 | tf_op jit(solution)/shard_map/all_gather | solution.py:121
  91.1 7.7 %fusion.26 = f32[1024,1024]{1,0:T(8,128)S(1)} fusion(bf16[1024,2048]{1,0:T(8,128)(2,1)} %bitcast.115, bf16[1,2048,1024]{2,1,0:T(8,128)(2,1)} %param.30), kind=kOutput, calls=%fused_computation.30 | convolution fusion | flops 4294967296 | bytes 12582912 | tf_op jit(solution)/shard_map/dot_general | solution.py:124
  98.8 5.4 %multiply_convert_fusion = bf16[1024,1024]{1,0:T(8,128)(2,1)S(1)} fusion(f32[1024,1024]{1,0:T(8,128)S(1)} %fusion.26, bf16[1024,2048]{1,0:T(8,128)(2,1)S(1)} %bitcast.116, bf16[1,2048,1024]{2,1,0:T(8,128)(2,1)S(1)} %copy-done.11), kind=kOutput, calls=%fused_computation.34 | convolution fusion | flops 4301258752 | bytes 14680064 | tf_op jit(solution)/shard_map/dot_general | solution.py:123
  104.2 6.1 %fusion.30 = bf16[8,128,2048]{2,1,0:T(8,128)(2,1)} fusion(bf16[8,128,1024]{2,1,0:T(8,128)(2,1)S(1)} %bitcast.117, bf16[1,1024,2048]{2,1,0:T(8,128)(2,1)S(1)} %copy-done.12), kind=kOutput, calls=%fused_computation.35 | convolution fusion | flops 4297064448 | bytes 10485760 | tf_op jit(solution)/shard_map/dot_general | solution.py:126
  112.0 30.3 %all-gather.5.cloned.1.call-done = bf16[2048,512]{1,0:T(8,128)(2,1)} async-done(((bf16[256,512]{1,0:T(8,128)(2,1)}), bf16[2048,512]{1,0:T(8,128)(2,1)}) %all-gather.5.cloned.1.call-update) | async-done | bytes 2097168 | tf_op jit(solution)/shard_map/all_gather | solution.py:28
  142.4 8.9 %reshape.193 = bf16[4,512,4,2,64]{4,3,2,1,0:T(2,128)(2,1)} reshape(bf16[2048,512]{1,0:T(8,128)(2,1)} %all-gather.5.cloned.1.call-done) | data formatting | bytes 4194304 | tf_op jit(solution)/shard_map/reshape | solution.py:33
  151.2 10.6 %copy.37 = bf16[4,512,4,2,64]{1,4,3,2,0:T(8,128)(2,1)} copy(bf16[4,512,4,2,64]{4,3,2,1,0:T(2,128)(2,1)} %reshape.193) | data formatting | bytes 4194304
  161.8 30.3 %all-gather.7.cloned.1.call-done = bf16[2048,512]{1,0:T(8,128)(2,1)} async-done(((bf16[256,512]{1,0:T(8,128)(2,1)}), bf16[2048,512]{1,0:T(8,128)(2,1)}) %all-gather.7.cloned.1.call-update) | async-done | bytes 2097168 | tf_op jit(solution)/shard_map/all_gather | solution.py:29
  192.2 4.0 %reshape.160 = bf16[4,512,4,128]{3,2,1,0:T(4,128)(2,1)} reshape(bf16[2048,512]{1,0:T(8,128)(2,1)} %all-gather.7.cloned.1.call-done) | data formatting | bytes 4194304 | tf_op jit(solution)/shard_map/reshape | solution.py:34
  196.2 4.4 %copy.38 = bf16[4,512,4,128]{1,3,2,0:T(8,128)(2,1)} copy(bf16[4,512,4,128]{3,2,1,0:T(4,128)(2,1)} %reshape.160) | data formatting | bytes 4194304
  201.2 15.2 %while.15 = (s32[]{:T(128)}, f32[256,4,2]{0,2,1:T(2,128)S(1)}, f32[256,4,2]{0,2,1:T(2,128)S(1)}, f32[256,4,2,128]{0,3,2,1:T(8,128)S(1)}, s32[4]{0:T(128)}, /*ind...) while((s32[]{:T(128)}, f32[256,4,2]{0,2,1:T(2,128)S(1)}, ...), condition=%wide.region_5.6_spmd.clone, body=%wide.region_0.5_spmd.clone.sunk | while | flops 416944896 | bytes 16654685 | solution.py:70
  201.2 1.2 dynamic_slice.27
  203.1 7.6 %conditional.3 = ((f32[256,4,2]{0,2,1:T(2,128)S(1)}, f32[256,4,2]{0,2,1:T(2,128)S(1)}, f32[256,4,2,128]{0,3,2,1:T(8,128)S(1)})) conditional(s32[]{:T(128)} %convert_element_type.73, (f32[256,4,2]{0,2,1:T(2,128)S(1)}, f32[256,4,2]{0,2,1:T(2,128)S(1)}, f32[256,4,2,128]{0,3,2,1:T(8,128)S(1)}) %tuple.44, (s32[]{:T(128)}, s32[]{:T(128)}, s32[]{:T(128)}, ...), branch_computations={%region_1.1_spmd, %region_2.4_spmd} | conditional | flops 416944896 | bytes 16653394 | solution.py:66
  205.2 1.9 fusion.2
  208.2 2.5 fusion.11
  210.7 1.2 dynamic_slice.27
  212.6 1.2 dynamic_slice.27
  218.5 19.1 %reduce-scatter.2.cloned.1.call-done = bf16[8,128,512]{2,1,0:T(8,128)(2,1)} async-done(((bf16[8,128,2048]{2,1,0:T(8,128)(2,1)}), bf16[8,128,512]{2,1,0:T(8,128)(2,1)}) %reduce-scatter.2.cloned.1.call-update) | async-done | bytes 1048592 | tf_op jit(solution)/shard_map/reduce_scatter | solution.py:130
  237.6 6.8 %all-to-all-start.1 = ((bf16[8,128,512]{2,1,0:T(8,128)(2,1)}), bf16[8,128,512]{2,1,0:T(8,128)(2,1)S(1)}, u32[]{:S(2)}, u32[]{:S(2)}) async-start(bf16[8,128,512]{2,1,0:T(8,128)(2,1)} %reduce-scatter.2.cloned.1.call-done), calls=%async_computation.2 | async-start | bytes 2097152 | tf_op jit(solution)/shard_map/all_to_all | solution.py:133
  244.7 11.9 %all-gather.9.cloned.1.call-done = bf16[256,2048]{0,1:T(8,128)(2,1)} async-done(((bf16[256,512]{0,1:T(8,128)(2,1)}), bf16[256,2048]{0,1:T(8,128)(2,1)}) %all-gather.9.cloned.1.call-update) | async-done | bytes 1048592 | tf_op jit(solution)/shard_map/all_gather | solution.py:81
  256.5 2.7 convolution_convert_fusion
  259.2 10.7 %all-to-all-done.1 = bf16[8,128,512]{2,1,0:T(8,128)(2,1)S(1)} async-done(((bf16[8,128,512]{2,1,0:T(8,128)(2,1)}), bf16[8,128,512]{2,1,0:T(8,128)(2,1)S(1)}, u32[]{:S(2)}, u32[]{:S(2)}) %all-to-all-start.1) | async-done | bytes 1048608 | tf_op jit(solution)/shard_map/all_to_all | solution.py:133
  269.9 2.6 gather_fusion.1
  272.5 1.7 reshape.165
  274.2 2.1 multiply_reduce_fusion
  (89 shorter events, 11.5 us)
Async XLA Ops:
  7.2 249.4 %copy-start = (bf16[2048,512]{1,0:T(8,128)(2,1)S(1)}, bf16[2048,512]{1,0:T(8,128)(2,1)}, u32[]{:S(2)}) copy-start(bf16[2048,512]{1,0:T(8,128)(2,1)} %param.23) | copy-start | bytes 6291460
  7.2 83.9 %all-gather.11.cloned.1.call-start = ((), (), s32[]{:S(2)}) async-start(), calls=%async_computation.6 | async-start | bytes 5242880 | tf_op jit(solution)/shard_map/all_gather | solution.py:121
  13.1 2.5 copy-start.7
  57.5 84.9 %all-gather.5.cloned.1.call-start = ((), (), s32[]{:S(2)}) async-start(), calls=%async_computation.3 | async-start | bytes 2359296 | tf_op jit(solution)/shard_map/all_gather | solution.py:28
  58.2 134.0 %all-gather.7.cloned.1.call-start = ((), (), s32[]{:S(2)}) async-start(), calls=%async_computation.4 | async-start | bytes 2359296 | tf_op jit(solution)/shard_map/all_gather | solution.py:29
  58.9 178.6 %reduce-scatter.2.cloned.1.call-start = ((), (), s32[]{:S(2)}) async-start(), calls=%async_computation.7 | async-start | bytes 5242880 | tf_op jit(solution)/shard_map/reduce_scatter | solution.py:130
  91.1 7.7 %copy-start.11 = (bf16[1,2048,1024]{2,1,0:T(8,128)(2,1)S(1)}, bf16[1,2048,1024]{2,1,0:T(8,128)(2,1)}, u32[]{:S(2)}) copy-start(bf16[1,2048,1024]{2,1,0:T(8,128)(2,1)} %param.29) | copy-start | bytes 12582916
  91.1 7.7 %copy-start.13 = (bf16[8,128,2048]{2,1,0:T(8,128)(2,1)S(1)}, bf16[8,128,2048]{2,1,0:T(8,128)(2,1)}, u32[]{:S(2)}) copy-start(bf16[8,128,2048]{2,1,0:T(8,128)(2,1)} %all-gather.11.cloned.1.call-done) | copy-start | bytes 12582916
  98.8 5.4 %copy-start.12 = (bf16[1,1024,2048]{2,1,0:T(8,128)(2,1)S(1)}, bf16[1,1024,2048]{2,1,0:T(8,128)(2,1)}, u32[]{:S(2)}) copy-start(bf16[1,1024,2048]{2,1,0:T(8,128)(2,1)} %param.31) | copy-start | bytes 12582916
  110.3 1.0 copy-start.1
  110.3 1.1 copy-start.9
  110.3 1.1 copy-start.10
  110.3 146.2 %all-gather.9.cloned.1.call-start = ((), (), s32[]{:S(2)}) async-start(), calls=%async_computation.5 | async-start | bytes 1310720 | tf_op jit(solution)/shard_map/all_gather | solution.py:81
  216.4 1.1 copy-start.4
  216.5 1.1 copy-start.5
  216.5 27.9 %copy-start.2 = (f32[256,2]{0,1:T(2,128)S(1)}, f32[256,2]{0,1:T(2,128)}, u32[]{:S(2)}) copy-start(f32[256,2]{0,1:T(2,128)} %param.27) | copy-start | bytes 6148
  216.5 27.9 %copy-start.3 = (f32[256,2]{0,1:T(2,128)S(1)}, f32[256,2]{0,1:T(2,128)}, u32[]{:S(2)}) copy-start(f32[256,2]{0,1:T(2,128)} %param.28) | copy-start | bytes 6148
  216.6 27.9 %copy-start.6 = (s32[256,2]{0,1:T(2,128)S(1)}, s32[256,2]{0,1:T(2,128)}, u32[]{:S(2)}) copy-start(s32[256,2]{0,1:T(2,128)} %get-tuple-element.168) | copy-start | bytes 6148
  216.6 28.0 %copy-start.8 = (s32[512,1]{0,1:T(1,128)S(1)}, s32[512,1]{0,1:T(1,128)}, u32[]{:S(2)}) copy-start(s32[512,1]{0,1:T(1,128)} %copy-done.7) | copy-start | bytes 6148
  237.6 32.3 %all-to-all-start.1 = ((bf16[8,128,512]{2,1,0:T(8,128)(2,1)}), bf16[8,128,512]{2,1,0:T(8,128)(2,1)S(1)}, u32[]{:S(2)}, u32[]{:S(2)}) async-start(bf16[8,128,512]{2,1,0:T(8,128)(2,1)} %reduce-scatter.2.cloned.1.call-done), calls=%async_computation.2 | async-start | bytes 2097152 | tf_op jit(solution)/shard_map/all_to_all | solution.py:133
Sparse Core Ops, SparseCore 0:
  57.6 33.4 all-gather.10
  93.2 49.0 all-gather.4
  144.5 47.6 all-gather.6
  194.6 42.9 reduce-scatter.1
  239.6 16.9 all-gather.8
where the time goes:
time: 284 us; the launch traced here: 283 us
  waiting for transfers between devices  136 us (48%)
  local copies, waits for them, and re-layouts  50.8 us (18%)
  blocking collectives  32.9 us (12%)
  matrix products  26.2 us (9%)
  between operations  14.1 us (5%)
  other arithmetic  11 us (4%)
  starting transfers between devices  7.14 us (3%)
  loops' own time  4.74 us (2%)
    all_to_all x1, blocking collectives, expert_block(): lax.all_to_all(own_columns, 'ep', split_axis=0, concat_axis=0, tiled=True)  32.9 us
    all_gather x1, waiting for transfers between devices, expert_block(): experts_arrived = lax.all_gather(arrived, 'tp', axis=2, tiled=True)  32.1 us
    all_gather x1, waiting for transfers between devices, token_mixer(): value_piece = lax.all_gather(values, 'ep', axis=0, tiled=True)  30.3 us
    all_gather x1, waiting for transfers between devices, token_mixer(): key_piece = lax.all_gather(key_rows, 'ep', axis=0, tiled=True)  30.3 us
    reduce_scatter x1, waiting for transfers between devices, expert_block(): lax.psum_scatter(partial_value.astype(jnp.bfloat16), 'tp', scatter_dimens...  19.1 us
    unnamed x32, local copies, waits for them, and re-layouts  16.7 us
    all_gather x1, waiting for transfers between devices, token_mixer(): lax.all_gather(head_out, 'tp', axis=1, tiled=True)  11.9 us
    all_to_all x1, waiting for transfers between devices, expert_block(): lax.all_to_all(answered, 'ep', split_axis=0, concat_axis=0, tiled=True)  10.7 us
  transfers between devices with their start and end apart: 6, of which 6 were waited for; matrix products, arithmetic and copies ran while one was open for 23% of the time, Pallas kernels for 0%

commit v1 on v0

--- a/solution.py
+++ b/solution.py
@@ -118,7 +118,12 @@
     columns = outgoing.shape[2] // lax.axis_size("tp")
     own_columns = lax.dynamic_slice_in_dim(outgoing, lax.axis_index("tp") * columns, columns, 2)
     arrived = lax.all_to_all(own_columns, "ep", split_axis=0, concat_axis=0, tiled=True)
-    experts_arrived = lax.all_gather(arrived, "tp", axis=2, tiled=True)
+    ring = [arrived]
+    for hop in range(3):
+        ring.append(lax.ppermute(ring[-1], "tp", [(dev, (dev + 1) % 4) for dev in range(4)]))
+    experts_arrived = jnp.roll(
+        jnp.concatenate(ring[::-1], axis=2), (lax.axis_index("tp") + 1) * ring[0].shape[2], axis=2
+    )
     stacked = experts_arrived.reshape(-1, experts_arrived.shape[2])
     gate_act = jnp.dot(stacked, gate_local, preferred_element_type=jnp.float32)
     up_act = jnp.dot(stacked, up_local, preferred_element_type=jnp.float32)

time: 284 us -> 245 us (0.86)
  waiting for transfers between devices: 136 us -> 100 us
  blocking collectives: 32.9 us -> 0 us
  starting transfers between devices: 7.14 us -> 32.7 us
  local copies, waits for them, and re-layouts: 50.8 us -> 57.7 us
  matrix products: 26.2 us -> 22.9 us
    ppermute x0 -> x3, waiting for transfers between devices: none -> 43 us  [expert_block(): lax.ppermute(ring[-1], 'tp', [(dev, (dev + 1) % 4) for dev in range(4)])]
    all_to_all x0 -> x1, waiting for transfers between devices: none -> 33.5 us  [expert_block(): lax.all_to_all(own_columns, 'ep', split_axis=0, concat_axis=0, tiled=True)]
    all_to_all x1 -> x0, blocking collectives: 32.9 us -> none  [expert_block(): lax.all_to_all(own_columns, 'ep', split_axis=0, concat_axis=0, tiled=True)]
    all_gather x1 -> x0, waiting for transfers between devices: 32.1 us -> none  [expert_block(): experts_arrived = lax.all_gather(arrived, 'tp', axis=2, tiled=True)]
    all_gather x1, waiting for transfers between devices: 30.3 us -> 0.01 us  [token_mixer(): value_piece = lax.all_gather(values, 'ep', axis=0, tiled=True)]
    all_gather x1, waiting for transfers between devices: 30.3 us -> 0.01 us  [token_mixer(): key_piece = lax.all_gather(key_rows, 'ep', axis=0, tiled=True)]
    reduce_scatter x1, waiting for transfers between devices: 19.1 us -> 0.41 us  [expert_block(): lax.psum_scatter(partial_value.astype(jnp.bfloat16), 'tp', scatter_dimens...]
    all_to_all x1, starting transfers between devices: 6.76 us -> 25.1 us  [expert_block(): lax.all_to_all(answered, 'ep', split_axis=0, concat_axis=0, tiled=True)]
  transfers between devices with their start and end apart: 6 -> 9, of which waited for: 6 -> 7; matrix products, arithmetic and copies ran while one was open for 23% -> 26% of each run, Pallas kernels for 0% -> 0%
where the time goes in v1:
time: 245 us; the launch traced here: 243 us
  waiting for transfers between devices  100 us (41%)
  local copies, waits for them, and re-layouts  57.7 us (24%)
  starting transfers between devices  32.7 us (13%)
  matrix products  22.9 us (9%)
  between operations  15.9 us (6%)
  other arithmetic  9.59 us (4%)
  loops' own time  4.29 us (2%)
    ppermute x3, waiting for transfers between devices, expert_block(): lax.ppermute(ring[-1], 'tp', [(dev, (dev + 1) % 4) for dev in range(4)])  43 us
    all_to_all x1, waiting for transfers between devices, expert_block(): lax.all_to_all(own_columns, 'ep', split_axis=0, concat_axis=0, tiled=True)  33.5 us
    unnamed x33, local copies, waits for them, and re-layouts  25.6 us
    all_to_all x1, starting transfers between devices, expert_block(): lax.all_to_all(answered, 'ep', split_axis=0, concat_axis=0, tiled=True)  25.1 us
    all_gather x1, waiting for transfers between devices, token_mixer(): lax.all_gather(head_out, 'tp', axis=1, tiled=True)  11.8 us
    all_to_all x1, waiting for transfers between devices, expert_block(): lax.all_to_all(answered, 'ep', split_axis=0, concat_axis=0, tiled=True)  10.6 us
    reshape x1, local copies, waits for them, and re-layouts, token_mixer(): key_blocks = key_piece.reshape(blocks, block_width, local_heads, 2, qk_size)  9.01 us
    all_to_all x1, starting transfers between devices, expert_block(): lax.all_to_all(own_columns, 'ep', split_axis=0, concat_axis=0, tiled=True)  7.28 us
  transfers between devices with their start and end apart: 9, of which 7 were waited for; matrix products, arithmetic and copies ran while one was open for 26% of the time, Pallas kernels for 0%

profile of v1, /device:TPU:0, one launch (start us, length us, event | category | flops | bytes accessed | tf_op | source)
XLA Modules:
  0.0 243.0 jit_solution(12737643492067361521)
XLA Ops:
  11.8 2.4 %scatter_custom_fusion = s32[1024]{0:T(1024)S(1)} fusion(s32[512]{0:T(512)S(1)} %bitcast.114, s32[512]{0:T(512)S(1)} %add_select_fusion, s32[]{:T(128)} %copy.74), kind=kCustom, calls=%fused_computation.85 | custom fusion | bytes 4100 | tf_op jit(solution)/shard_map/scatter | solution.py:113
  14.3 1.5 fusion.35
  15.8 1.5 fusion.37
  17.3 6.0 %gather_fusion = bf16[1024,2048]{1,0:T(8,128)(2,1)} fusion(bf16[256,2048]{1,0:T(8,128)(2,1)S(1)} %fusion.37, s32[1024]{0:T(1024)S(1)} %fusion.46), kind=kCustom, calls=%fused_computation | custom fusion | bytes 8392704 | tf_op jit(solution)/shard_map/gather | solution.py:114
  23.3 2.3 constant_dynamic-slice_fusion.1
  25.6 7.3 %all-to-all-start = ((bf16[8,128,512]{2,1,0:T(8,128)(2,1)}), bf16[8,128,512]{2,1,0:T(8,128)(2,1)S(1)}, u32[]{:S(2)}, u32[]{:S(2)}) async-start(bf16[8,128,512]{2,1,0:T(8,128)(2,1)} %constant_dynamic-slice_fusion.1), calls=%async_computation | async-start | bytes 2097152 | tf_op jit(solution)/shard_map/all_to_all | solution.py:120
  33.7 33.5 %all-to-all-done = bf16[8,128,512]{2,1,0:T(8,128)(2,1)S(1)} async-done(((bf16[8,128,512]{2,1,0:T(8,128)(2,1)}), bf16[8,128,512]{2,1,0:T(8,128)(2,1)S(1)}, u32[]{:S(2)}, u32[]{:S(2)}) %all-to-all-start) | async-done | bytes 1048608 | tf_op jit(solution)/shard_map/all_to_all | solution.py:120
  67.1 14.2 %collective-permute-done = bf16[8,128,512]{2,1,0:T(8,128)(2,1)S(1)} collective-permute-done((bf16[8,128,512]{2,1,0:T(8,128)(2,1)S(1)}, bf16[8,128,512]{2,1,0:T(8,128)(2,1)S(1)}, u32[]{:S(2)}, u32[]{:S(2)}) %collective-permute-start) | collective-permute-done | bytes 1048608 | tf_op jit(solution)/shard_map/ppermute | solution.py:123
  82.4 14.3 %collective-permute-done.1 = bf16[8,128,512]{2,1,0:T(8,128)(2,1)} collective-permute-done((bf16[8,128,512]{2,1,0:T(8,128)(2,1)S(1)}, bf16[8,128,512]{2,1,0:T(8,128)(2,1)}, u32[]{:S(2)}, u32[]{:S(2)}) %collective-permute-start.1) | collective-permute-done | bytes 1048608 | tf_op jit(solution)/shard_map/ppermute | solution.py:123
  96.8 14.4 %collective-permute-done.2 = bf16[8,128,512]{2,1,0:T(8,128)(2,1)} collective-permute-done((bf16[8,128,512]{2,1,0:T(8,128)(2,1)}, bf16[8,128,512]{2,1,0:T(8,128)(2,1)}, u32[]{:S(2)}, u32[]{:S(2)}) %collective-permute-start.2) | collective-permute-done | bytes 1048608 | tf_op jit(solution)/shard_map/ppermute | solution.py:123
  112.7 1.4 constant_dynamic-update-slice_fusion.6
  114.4 1.4 constant_dynamic-update-slice_fusion.3
  115.8 1.4 constant_dynamic-update-slice_fusion.2
  117.8 1.9 copy-done.8
  119.7 4.5 %fusion.28 = f32[1024,1024]{1,0:T(8,128)S(1)} fusion(bf16[1024,2048]{1,0:T(8,128)(2,1)S(1)} %bitcast.106, bf16[1,2048,1024]{2,1,0:T(8,128)(2,1)S(1)} %copy-done.8), kind=kOutput, calls=%fused_computation.32 | convolution fusion | flops 4294967296 | bytes 12582912 | tf_op jit(solution)/shard_map/dot_general | solution.py:128
  124.2 5.2 %multiply_convert_fusion = bf16[1024,1024]{1,0:T(8,128)(2,1)S(1)} fusion(f32[1024,1024]{1,0:T(8,128)S(1)} %fusion.28, bf16[1024,2048]{1,0:T(8,128)(2,1)S(1)} %bitcast.107, bf16[1,2048,1024]{2,1,0:T(8,128)(2,1)S(1)} %copy-done.9), kind=kOutput, calls=%fused_computation.34 | convolution fusion | flops 4301258752 | bytes 14680064 | tf_op jit(solution)/shard_map/dot_general | solution.py:129
  129.4 6.1 %fusion.30 = bf16[8,128,2048]{2,1,0:T(8,128)(2,1)} fusion(bf16[8,128,1024]{2,1,0:T(8,128)(2,1)S(1)} %bitcast.117, bf16[1,1024,2048]{2,1,0:T(8,128)(2,1)S(1)} %copy-done.10), kind=kOutput, calls=%fused_computation.35 | convolution fusion | flops 4297064448 | bytes 10485760 | tf_op jit(solution)/shard_map/dot_general | solution.py:131
  136.7 9.0 %reshape.193 = bf16[4,512,4,2,64]{4,3,2,1,0:T(2,128)(2,1)} reshape(bf16[2048,512]{1,0:T(8,128)(2,1)} %all-gather.4.cloned.1.call-done) | data formatting | bytes 4194304 | tf_op jit(solution)/shard_map/reshape | solution.py:33
  145.7 10.7 %copy.37 = bf16[4,512,4,2,64]{1,4,3,2,0:T(8,128)(2,1)} copy(bf16[4,512,4,2,64]{4,3,2,1,0:T(2,128)(2,1)} %reshape.193) | data formatting | bytes 4194304
  156.4 4.0 %reshape.160 = bf16[4,512,4,128]{3,2,1,0:T(4,128)(2,1)} reshape(bf16[2048,512]{1,0:T(8,128)(2,1)} %all-gather.6.cloned.1.call-done) | data formatting | bytes 4194304 | tf_op jit(solution)/shard_map/reshape | solution.py:34
  160.4 4.3 %copy.38 = bf16[4,512,4,128]{1,3,2,0:T(8,128)(2,1)} copy(bf16[4,512,4,128]{3,2,1,0:T(4,128)(2,1)} %reshape.160) | data formatting | bytes 4194304
  164.8 12.3 %while.15 = (s32[]{:T(128)}, f32[256,4,2]{0,2,1:T(2,128)S(1)}, f32[256,4,2]{0,2,1:T(2,128)S(1)}, f32[256,4,2,128]{0,3,2,1:T(8,128)S(1)}, s32[4]{0:T(128)S(1)}, /...) while((s32[]{:T(128)}, f32[256,4,2]{0,2,1:T(2,128)S(1)}, ...), condition=%wide.region_5.6_spmd.clone, body=%wide.region_0.5_spmd.clone.sunk | while | flops 416944896 | bytes 16654677 | solution.py:70
  166.0 7.4 %conditional.3 = ((f32[256,4,2]{0,2,1:T(2,128)S(1)}, f32[256,4,2]{0,2,1:T(2,128)S(1)}, f32[256,4,2,128]{0,3,2,1:T(8,128)S(1)})) conditional(s32[]{:T(128)} %convert_element_type.73, (f32[256,4,2]{0,2,1:T(2,128)S(1)}, f32[256,4,2]{0,2,1:T(2,128)S(1)}, f32[256,4,2,128]{0,3,2,1:T(8,128)S(1)}) %tuple.44, (s32[]{:T(128)}, s32[]{:T(128)}, s32[]{:T(128)}, ...), branch_computations={%region_1.1_spmd, %region_2.4_spmd} | conditional | flops 416944896 | bytes 16653394 | solution.py:66
  167.9 1.9 fusion.2
  170.9 2.5 %fusion.11 = f32[256,4,2,128]{0,3,2,1:T(8,128)S(1)} fusion(f32[4,2,512,256]{3,2,1,0:T(8,128)S(1)} %get-tuple-element.165, f32[256,4,2]{0,2,1:T(2,128)S(1)} %max.2, pred[256,512]{0,1:T(8,128)(4,1)S(1)} %broadcast_compare_fusion, f32[256,4,2,128]{0,3,2,1:T(8,128)S(1)} %get-tuple-element.71, bf16[4,512,4,128]{1,3,2,0:T(8,128)(2,1)} %get-tuple-element.72, ...), kind=kOutput, calls=%fused_computation.12 | convolution fusion | flops 274202624 | bytes 6963204 | tf_op jit(solution)/shard_map/while/body/eval_jaxpr/cond/branch_1_fun/qhmk,khe->qhme/dot_general | solution.py:57
  178.8 25.1 %all-to-all-start.1 = ((bf16[8,128,512]{2,1,0:T(8,128)(2,1)}), bf16[8,128,512]{2,1,0:T(8,128)(2,1)S(1)}, u32[]{:S(2)}, u32[]{:S(2)}) async-start(bf16[8,128,512]{2,1,0:T(8,128)(2,1)} %reduce-scatter.2.cloned.1.call-done), calls=%async_computation.2 | async-start | bytes 2097152 | tf_op jit(solution)/shard_map/all_to_all | solution.py:138
  204.2 11.8 %all-gather.8.cloned.1.call-done = bf16[256,2048]{0,1:T(8,128)(2,1)} async-done(((bf16[256,512]{0,1:T(8,128)(2,1)}), bf16[256,2048]{0,1:T(8,128)(2,1)}) %all-gather.8.cloned.1.call-update) | async-done | bytes 1048592 | tf_op jit(solution)/shard_map/all_gather | solution.py:81
  216.0 2.7 %convolution_convert_fusion = bf16[256,512]{1,0:T(8,128)(2,1)} fusion(bf16[256,2048]{0,1:T(8,128)(2,1)} %all-gather.8.cloned.1.call-done, bf16[2048,512]{1,0:T(8,128)(2,1)S(1)} %copy-done), kind=kOutput, calls=%fused_computation.41 | convolution fusion | flops 537001984 | bytes 3407872 | tf_op jit(solution)/shard_map/dot_general | solution.py:80
  218.6 10.6 %all-to-all-done.1 = bf16[8,128,512]{2,1,0:T(8,128)(2,1)S(1)} async-done(((bf16[8,128,512]{2,1,0:T(8,128)(2,1)}), bf16[8,128,512]{2,1,0:T(8,128)(2,1)S(1)}, u32[]{:S(2)}, u32[]{:S(2)}) %all-to-all-start.1) | async-done | bytes 1048608 | tf_op jit(solution)/shard_map/all_to_all | solution.py:138
  229.2 2.6 %gather_fusion.1 = bf16[512,512]{1,0:T(8,128)(2,1)} fusion(bf16[1024,512]{1,0:T(8,128)(2,1)S(1)} %bitcast.103, s32[1024]{0:T(1024)S(1)} %pad_clamp_fusion), kind=kCustom, calls=%fused_computation.1 | custom fusion | bytes 1050624 | tf_op jit(solution)/shard_map/gather | solution.py:139
  231.9 1.7 reshape.165
  233.6 2.1 multiply_reduce_fusion
  (96 shorter events, 14.7 us)
Async XLA Ops:
  8.0 208.0 %copy-start = (bf16[2048,512]{1,0:T(8,128)(2,1)S(1)}, bf16[2048,512]{1,0:T(8,128)(2,1)}, u32[]{:S(2)}) copy-start(bf16[2048,512]{1,0:T(8,128)(2,1)} %param.23) | copy-start | bytes 6291460
  25.6 41.5 %all-to-all-start = ((bf16[8,128,512]{2,1,0:T(8,128)(2,1)}), bf16[8,128,512]{2,1,0:T(8,128)(2,1)S(1)}, u32[]{:S(2)}, u32[]{:S(2)}) async-start(bf16[8,128,512]{2,1,0:T(8,128)(2,1)} %constant_dynamic-slice_fusion.1), calls=%async_computation | async-start | bytes 2097152 | tf_op jit(solution)/shard_map/all_to_all | solution.py:120
  32.9 103.8 %all-gather.4.cloned.1.call-start = ((), (), s32[]{:S(2)}) async-start(), calls=%async_computation.3 | async-start | bytes 2359296 | tf_op jit(solution)/shard_map/all_gather | solution.py:28
  33.6 122.8 %all-gather.6.cloned.1.call-start = ((), (), s32[]{:S(2)}) async-start(), calls=%async_computation.4 | async-start | bytes 2359296 | tf_op jit(solution)/shard_map/all_gather | solution.py:29
  67.1 14.2 %collective-permute-start = (bf16[8,128,512]{2,1,0:T(8,128)(2,1)S(1)}, bf16[8,128,512]{2,1,0:T(8,128)(2,1)S(1)}, u32[]{:S(2)}, u32[]{:S(2)}) collective-permute-start(bf16[8,128,512]{2,1,0:T(8,128)(2,1)S(1)} %all-to-all-done), channel_id=1, source_target_pairs={{0,1},{1,2},{2,3},{3,0},{4,5},{5,6},{6,7},{7,4},{8,9},{9,10},{10,1... | collective-permute-start | bytes 3145736 | tf_op jit(solution)/shard_map/ppermute | solution.py:123
  81.4 1.0 copy-start.1
  82.4 14.3 %collective-permute-start.1 = (bf16[8,128,512]{2,1,0:T(8,128)(2,1)S(1)}, bf16[8,128,512]{2,1,0:T(8,128)(2,1)}, u32[]{:S(2)}, u32[]{:S(2)}) collective-permute-start(bf16[8,128,512]{2,1,0:T(8,128)(2,1)S(1)} %collective-permute-done), channel_id=1, source_target_pairs={{0,1},{1,2},{2,3},{3,0},{4,5},{5,6},{6,7},{7,4},{8,9},{9,10},{10,1... | collective-permute-start | bytes 3145736 | tf_op jit(solution)/shard_map/ppermute | solution.py:123
  96.7 14.5 %collective-permute-start.2 = (bf16[8,128,512]{2,1,0:T(8,128)(2,1)}, bf16[8,128,512]{2,1,0:T(8,128)(2,1)}, u32[]{:S(2)}, u32[]{:S(2)}) collective-permute-start(bf16[8,128,512]{2,1,0:T(8,128)(2,1)} %collective-permute-done.1), channel_id=1, source_target_pairs={{0,1},{1,2},{2,3},{3,0},{4,5},{5,6},{6,7},{7,4},{8,9},{9,10},{10,1... | collective-permute-start | bytes 3145736 | tf_op jit(solution)/shard_map/ppermute | solution.py:123
  96.8 82.0 %reduce-scatter.2.cloned.1.call-start = ((), (), s32[]{:S(2)}) async-start(), calls=%async_computation.6 | async-start | bytes 5242880 | tf_op jit(solution)/shard_map/reduce_scatter | solution.py:135
  96.8 17.2 %copy-start.2 = (bf16[8,128,512]{2,1,0:T(8,128)(2,1)S(1)}, bf16[8,128,512]{2,1,0:T(8,128)(2,1)}, u32[]{:S(2)}) copy-start(bf16[8,128,512]{2,1,0:T(8,128)(2,1)} %copy-done.1) | copy-start | bytes 3145732
  117.5 2.2 copy-start.8
  119.7 4.5 %copy-start.9 = (bf16[1,2048,1024]{2,1,0:T(8,128)(2,1)S(1)}, bf16[1,2048,1024]{2,1,0:T(8,128)(2,1)}, u32[]{:S(2)}) copy-start(bf16[1,2048,1024]{2,1,0:T(8,128)(2,1)} %param.30) | copy-start | bytes 12582916
  124.2 5.2 %copy-start.10 = (bf16[1,1024,2048]{2,1,0:T(8,128)(2,1)S(1)}, bf16[1,1024,2048]{2,1,0:T(8,128)(2,1)}, u32[]{:S(2)}) copy-start(bf16[1,1024,2048]{2,1,0:T(8,128)(2,1)} %param.31) | copy-start | bytes 12582916
  135.5 0.9 copy-start.3
  135.5 1.1 copy-start.6
  135.5 1.1 copy-start.7
  135.6 80.4 %all-gather.8.cloned.1.call-start = ((), (), s32[]{:S(2)}) async-start(), calls=%async_computation.5 | async-start | bytes 1310720 | tf_op jit(solution)/shard_map/all_gather | solution.py:81
  177.1 26.8 %copy-start.4 = (f32[256,2]{0,1:T(2,128)S(1)}, f32[256,2]{0,1:T(2,128)}, u32[]{:S(2)}) copy-start(f32[256,2]{0,1:T(2,128)} %param.27) | copy-start | bytes 6148
  177.1 26.8 %copy-start.5 = (f32[256,2]{0,1:T(2,128)S(1)}, f32[256,2]{0,1:T(2,128)}, u32[]{:S(2)}) copy-start(f32[256,2]{0,1:T(2,128)} %param.28) | copy-start | bytes 6148
  178.8 50.5 %all-to-all-start.1 = ((bf16[8,128,512]{2,1,0:T(8,128)(2,1)}), bf16[8,128,512]{2,1,0:T(8,128)(2,1)S(1)}, u32[]{:S(2)}, u32[]{:S(2)}) async-start(bf16[8,128,512]{2,1,0:T(8,128)(2,1)} %reduce-scatter.2.cloned.1.call-done), calls=%async_computation.2 | async-start | bytes 2097152 | tf_op jit(solution)/shard_map/all_to_all | solution.py:138
Sparse Core Ops, SparseCore 0:
  35.8 58.0 all-gather.3
  96.9 48.1 all-gather.5
Sparse Core Ops, SparseCore 1:
  135.7 43.1 reduce-scatter.1
  180.8 35.1 all-gather.7
